TPU v7x, 32 devices: a whole 2x2x4 slice. The times are simulated.
32 devices in a mesh: ep: 8 (over z, y), tp: 4 (over x, core).
Axes of the slice: x: 2, y: 2, z: 4, core: 2. Of those that a mesh axis runs over, the one named last changes fastest.
Arguments:
- tokens: bfloat16 [6144, 2048], P('ep')
- in_gain: float32 [2048], replicated, may hold values from 0.1 to 1.9
- route_ids: int32 [6144, 2], P('ep'), may hold values from 0 to 7, all different within a row; in each aligned block of 768 rows (0 to 767, 768 to 1535, ...) at most 384 rows name the same one
- route_scores: float32 [6144, 2], P('ep'), may hold values from 0.1 to 1
- gate_weight: bfloat16 [8, 2048, 1024], P('ep', None, 'tp'), may hold values from -0.125 to 0.125
- up_weight: bfloat16 [8, 2048, 1024], P('ep', None, 'tp'), may hold values from -0.125 to 0.125
- down_weight: bfloat16 [8, 1024, 2048], P('ep', 'tp')
- out_gain: float32 [2048], P('tp'), may hold values from 0.1 to 1.9
Outputs:
- mixed: bfloat16 [6144, 2048], P('ep', 'tp')
Inputs may be any that keep to these rules, and one draw needn't show every extreme that they name: `route_ids`: each row names 2 different experts. Among the rows of one index of ep (aligned blocks of 768 rows) no expert is named more than 384 times, a bound that some block reaches.
All inputs are finite; a program needn't handle non-finite values.
Results may differ from a plain program's by a relative error of at most 0.012.
Values may be sent and summed in bfloat16 or wider, within the bound.
A program may use at most 128 MiB of HBM per device.

v0:
```python
import jax
import jax.numpy as jnp
from jax import lax
from jax.sharding import PartitionSpec as P

epsilon = 1e-06


def per_device(
    tokens, in_gain, route_ids, route_scores, gate_weight, up_weight, down_weight, out_gain
):
    count_ep = lax.axis_size("ep")
    count_tp = lax.axis_size("tp")
    local_experts = gate_weight.shape[0]
    experts = count_ep * local_experts
    tok_count, full_width = tokens.shape
    choose_count = route_ids.shape[1]
    capacity = 2 * tok_count * choose_count // experts
    part_width = full_width // count_tp
    as_float = tokens.astype(jnp.float32)
    normed = (
        as_float
        * lax.rsqrt(jnp.mean(as_float * as_float, axis=1, keepdims=True) + epsilon)
        * in_gain
    ).astype(jnp.bfloat16)
    flat_ids = route_ids.reshape(-1)
    one_hot = (flat_ids[:, None] == jnp.arange(experts, dtype=jnp.int32)[None, :]).astype(jnp.int32)
    slot_index = jnp.sum((jnp.cumsum(one_hot, axis=0) - 1) * one_hot, axis=1)
    row_index = jnp.arange(tok_count * choose_count, dtype=jnp.int32) // choose_count
    own_slice = lax.dynamic_slice_in_dim(normed, lax.axis_index("tp") * part_width, part_width, 1)
    buffer = jnp.zeros((experts, capacity, part_width), jnp.bfloat16)
    buffer = buffer.at[flat_ids, slot_index].set(own_slice[row_index])
    buffer = buffer.reshape(count_ep, local_experts, capacity, part_width)
    received = lax.all_to_all(buffer, "ep", split_axis=0, concat_axis=0, tiled=True)
    piece = lax.all_gather(received, "tp", axis=3, tiled=True)
    gate_add = jnp.einsum("secn,enf->secf", piece, gate_weight, preferred_element_type=jnp.float32)
    up_add = jnp.einsum("secn,enf->secf", piece, up_weight, preferred_element_type=jnp.float32)
    hidden = (jax.nn.silu(gate_add) * up_add).astype(jnp.bfloat16)
    partial_terms = jnp.einsum(
        "secf,efd->secd", hidden, down_weight, preferred_element_type=jnp.float32
    ).astype(jnp.bfloat16)
    summed = (
        lax.psum_scatter(partial_terms, "tp", scatter_dimension=3, tiled=True)
        .astype(jnp.float32)
        .astype(jnp.bfloat16)
    )
    returned = lax.all_to_all(summed, "ep", split_axis=0, concat_axis=0, tiled=True).reshape(
        experts, capacity, part_width
    )
    picked = (
        returned[flat_ids, slot_index]
        .astype(jnp.float32)
        .reshape(tok_count, choose_count, part_width)
    )
    mix_weight = route_scores / jnp.sum(route_scores, axis=1, keepdims=True)
    combined = jnp.sum(mix_weight[:, :, None] * picked, axis=1)
    squares_sum = lax.psum(jnp.sum(combined * combined, axis=1), "tp")
    scaled = combined * lax.rsqrt(squares_sum[:, None] / full_width + epsilon) * out_gain
    return scaled.astype(jnp.bfloat16)


def solution(mesh):
    in_specs = (
        P("ep", None),
        P(),
        P("ep", None),
        P("ep", None),
        P("ep", None, "tp"),
        P("ep", None, "tp"),
        P("ep", "tp", None),
        P("tp"),
    )
    out_specs = P("ep", "tp")
    return jax.shard_map(
        per_device, mesh=mesh, in_specs=in_specs, out_specs=out_specs, check_vma=False
    )
```

profile of v0, /device:TPU:0, one launch (start us, length us, event | category | flops | bytes accessed | tf_op | source)
XLA Modules:
  0.0 441.9 jit_solution(14998475770619304312)
XLA Ops:
  6.5 1.0 copy.15
  7.5 0.2 eq.29
  7.7 0.2 eq.25
  8.0 0.2 reshape.152
  8.2 5.5 %convert_element_type.39 = f32[768,2048]{1,0:T(8,128)} convert(bf16[768,2048]{1,0:T(8,128)(2,1)} %param.8) | non-fusion elementwise | flops 1572864 | bytes 9437184 | tf_op jit(solution)/shard_map/convert_element_type | solution.py:20
  13.8 0.7 multiply_reduce_fusion
  14.5 2.3 reduce-window.6
  16.8 0.3 slice_reduce_fusion
  17.7 0.8 dynamic-slice
  18.5 1.6 fusion.11
  20.1 16.3 %scatter_custom_fusion = bf16[3072,512]{1,0:T(8,128)(2,1)} fusion(s32[1536]{0:T(1024)S(1)} %broadcast_select_fusion, bf16[768,512]{1,0:T(8,128)(2,1)S(1)} %fusion.11, s32[2048]{0:T(1024)S(1)} %pad_clamp_fusion, bf16[]{:T(256)} %constant.38.clone.1), kind=kCustom, calls=%fused_computation.21 | custom fusion | bytes 3145730
  36.4 78.1 %all_to_all.10 = bf16[8,1,384,512]{3,2,1,0:T(8,128)(2,1)} all-to-all(bf16[8,1,384,512]{3,2,1,0:T(8,128)(2,1)} %bitcast.86), channel_id=1, replica_groups=mesh['ep'=8,'tp'=4] {'ep'}, dimensions={0} | all-to-all | bytes 6291456 | tf_op jit(solution)/shard_map/all_to_all | solution.py:34
  114.6 0.2 reduce-scatter.2.cloned.1.call-start
  114.8 81.0 %all-gather.2.cloned.1.call-done = bf16[8,1,384,2048]{3,2,0,1:T(8,128)(2,1)} async-done(((bf16[8,1,384,512]{3,2,0,1:T(8,128)(2,1)}), bf16[8,1,384,2048]{3,2,0,1:T(8,128)(2,1)}) %all-gather.2.cloned.1.call-update) | async-done | bytes 12582928 | tf_op jit(solution)/shard_map/all_gather | solution.py:35
  195.8 9.8 %fusion.2 = f32[8,384,256]{2,1,0:T(8,128)} fusion(bf16[8,1,384,2048]{3,2,0,1:T(8,128)(2,1)} %all-gather.2.cloned.1.call-done, bf16[1,2048,256]{2,1,0:T(8,128)(2,1)S(1)} %copy-done.6), kind=kOutput, calls=%fused_computation.5 | convolution fusion | flops 3221225472 | bytes 16777216 | tf_op jit(solution)/shard_map/secn,enf->secf/dot_general | solution.py:36
  205.6 18.8 %convert_bitcast_fusion = bf16[8,1,384,2048]{3,2,0,1:T(8,128)(2,1)} fusion(f32[8,384,256]{2,1,0:T(8,128)} %fusion.2, bf16[8,1,384,2048]{3,2,0,1:T(8,128)(2,1)} %all-gather.2.cloned.1.call-done, bf16[1,256,2048]{2,1,0:T(8,128)(2,1)S(1)} %copy-done, bf16[1,2048,256]{2,1,0:T(8,128)(2,1)S(1)} %copy-done.7), kind=kOutput, calls=%fused_computation.7 | convolution fusion | flops 6453460992 | bytes 30408704 | tf_op jit(solution)/shard_map/secf,efd->secd/dot_general | solution.py:39
  224.4 97.3 %reduce-scatter.2.cloned.1.call-done = bf16[8,1,384,512]{3,2,0,1:T(8,128)(2,1)} async-done(((bf16[8,1,384,2048]{3,2,0,1:T(8,128)(2,1)}), bf16[8,1,384,512]{3,2,0,1:T(8,128)(2,1)}) %reduce-scatter.2.cloned.1.call-update) | async-done | bytes 3145744 | tf_op jit(solution)/shard_map/reduce_scatter | solution.py:43
  321.7 5.6 %all-to-all-start.1 = ((bf16[8,1,384,512]{3,2,1,0:T(8,128)(2,1)}), bf16[8,1,384,512]{3,2,1,0:T(8,128)(2,1)}, u32[]{:S(2)}, u32[]{:S(2)}) async-start(bf16[8,1,384,512]{3,2,1,0:T(8,128)(2,1)} %bitcast.87), calls=%async_computation.2 | async-start | bytes 6291456 | tf_op jit(solution)/shard_map/all_to_all | solution.py:47
  327.6 70.4 %all-to-all-done.1 = bf16[8,1,384,512]{3,2,1,0:T(8,128)(2,1)} async-done(((bf16[8,1,384,512]{3,2,1,0:T(8,128)(2,1)}), bf16[8,1,384,512]{3,2,1,0:T(8,128)(2,1)}, u32[]{:S(2)}, u32[]{:S(2)}) %all-to-all-start.1) | async-done | bytes 3145760 | tf_op jit(solution)/shard_map/all_to_all | solution.py:47
  398.0 20.5 %gather_fusion = bf16[1536,512]{1,0:T(8,128)(2,1)S(1)} fusion(bf16[8,384,512]{2,1,0:T(8,128)(2,1)} %bitcast.23, s32[1536]{0:T(1024)S(1)} %get-tuple-element.5), kind=kCustom, calls=%fused_computation.1 | custom fusion | bytes 3158016 | tf_op jit(solution)/shard_map/gather | solution.py:51
  418.5 3.3 reshape.166
  421.8 6.0 %multiply_reduce_fusion.1 = f32[768,512]{1,0:T(8,128)S(1)} fusion(f32[768,2,512]{2,1,0:T(2,128)} %reshape.166, f32[768,2]{1,0:T(8,128)S(1)} %copy.14), kind=kLoop, calls=%fused_computation.16 | loop fusion | flops 1179648 | bytes 4724736 | tf_op jit(solution)/shard_map/reduce_sum | solution.py:56
  428.0 6.0 %psum.7 = f32[768]{0:T(1024)S(1)} all-reduce(f32[768]{0:T(1024)S(1)} %multiply_reduce_fusion.2), channel_id=1, replica_groups=mesh['ep'=8,'tp'=4] {'tp'}, use_global_device_ids=true, to_apply=%region_9.10 | all-reduce | flops 768 | bytes 6144 | tf_op jit(solution)/shard_map/psum | solution.py:57
  434.0 1.1 multiply_convert_fusion
  (35 shorter events, 1.1 us)
Async XLA Ops:
  6.5 199.1 %copy-start = (bf16[1,256,2048]{2,1,0:T(8,128)(2,1)S(1)}, bf16[1,256,2048]{2,1,0:T(8,128)(2,1)}, u32[]{:S(2)}) copy-start(bf16[1,256,2048]{2,1,0:T(8,128)(2,1)} %param.14) | copy-start | bytes 3145732
  6.5 189.3 %all-gather.2.cloned.1.call-start = ((), (), s32[]{:S(2)}) async-start(), calls=%async_computation.3 | async-start | bytes 15728640 | tf_op jit(solution)/shard_map/all_gather | solution.py:35
  8.2 5.6 %copy-start.1 = (bf16[768,2048]{1,0:T(8,128)(2,1)S(1)}, bf16[768,2048]{1,0:T(8,128)(2,1)}, u32[]{:S(2)}) copy-start(bf16[768,2048]{1,0:T(8,128)(2,1)} %param.8) | copy-start | bytes 9437188
  13.8 3.7 copy-start.5
  13.8 3.8 copy-start.4
  114.5 81.3 %copy-start.6 = (bf16[1,2048,256]{2,1,0:T(8,128)(2,1)S(1)}, bf16[1,2048,256]{2,1,0:T(8,128)(2,1)}, u32[]{:S(2)}) copy-start(bf16[1,2048,256]{2,1,0:T(8,128)(2,1)} %param.12) | copy-start | bytes 3145732
  114.6 91.0 %copy-start.7 = (bf16[1,2048,256]{2,1,0:T(8,128)(2,1)S(1)}, bf16[1,2048,256]{2,1,0:T(8,128)(2,1)}, u32[]{:S(2)}) copy-start(bf16[1,2048,256]{2,1,0:T(8,128)(2,1)} %param.13) | copy-start | bytes 3145732
  114.6 207.2 %reduce-scatter.2.cloned.1.call-start = ((), (), s32[]{:S(2)}) async-start(), calls=%async_computation.4 | async-start | bytes 15728640 | tf_op jit(solution)/shard_map/reduce_scatter | solution.py:43
  321.7 5.6 %copy-start.2 = (f32[768,2]{0,1:T(2,128)S(1)}, f32[768,2]{0,1:T(2,128)}, u32[]{:S(2)}) copy-start(f32[768,2]{0,1:T(2,128)} %param.11) | copy-start | bytes 18436
  321.7 76.3 %all-to-all-start.1 = ((bf16[8,1,384,512]{3,2,1,0:T(8,128)(2,1)}), bf16[8,1,384,512]{3,2,1,0:T(8,128)(2,1)}, u32[]{:S(2)}, u32[]{:S(2)}) async-start(bf16[8,1,384,512]{3,2,1,0:T(8,128)(2,1)} %bitcast.87), calls=%async_computation.2 | async-start | bytes 6291456 | tf_op jit(solution)/shard_map/all_to_all | solution.py:47
  421.8 12.2 %copy-start.3 = (f32[512]{0:T(512)S(1)}, f32[512]{0:T(512)}, u32[]{:S(2)}) copy-start(f32[512]{0:T(512)} %param.15) | copy-start | bytes 6148
Sparse Core Ops, SparseCore 0:
  114.7 81.0 all-gather.1
  224.5 97.1 reduce-scatter.1
where the time goes:
time: 443 us; the launch traced here: 442 us
  waiting for transfers between devices  249 us (56%)
  blocking collectives  84.1 us (19%)
  local copies, waits for them, and re-layouts  43.1 us (10%)
  matrix products  28.6 us (6%)
  other arithmetic  18 us (4%)
  between operations  13.6 us (3%)
  starting transfers between devices  5.85 us (1%)
    reduce_scatter x1, waiting for transfers between devices, per_device(): lax.psum_scatter(partial_terms, 'tp', scatter_dimension=3, tiled=True)  97.3 us
    all_gather x1, waiting for transfers between devices, per_device(): piece = lax.all_gather(received, 'tp', axis=3, tiled=True)  81 us
    all_to_all x1, blocking collectives, per_device(): lax.all_to_all(buffer, 'ep', split_axis=0, concat_axis=0, tiled=True)  78.1 us
    all_to_all x1, waiting for transfers between devices, per_device(): lax.all_to_all(summed, 'ep', split_axis=0, concat_axis=0, tiled=True)  70.4 us
    gather x1, local copies, waits for them, and re-layouts, per_device(): returned[flat_ids, slot_index].astype(jnp.float32)  20.5 us
    dot_general x1, matrix products, per_device(): jnp.einsum('secf,efd->secd', hidden, down_weight, preferred_element_type=...  18.8 us
    unnamed x18, local copies, waits for them, and re-layouts  17.3 us
    dot_general x1, matrix products, per_device(): jnp.einsum('secn,enf->secf', piece, gate_weight, preferred_element_type=j...  9.79 us
  transfers between devices with their start and end apart: 3, of which 3 were waited for; matrix products, arithmetic and copies ran while one was open for 0% of the time, Pallas kernels for 0%

commit v1 on v0

v1 whole, which is shorter than its diff:
```python
import jax
import jax.numpy as jnp
from jax import lax
from jax.sharding import PartitionSpec as P

epsilon = 1e-06


def gathered(block, count):
    blocks = [block]
    bit = 1
    swaps = []
    while bit < count:
        swaps.append([(i, i ^ bit) for i in range(count)])
        bit *= 2
    first = lax.ppermute(block, "tp", swaps[0])
    blocks.append(first)
    for pairs in swaps[1:]:
        far = lax.ppermute(block, "tp", pairs)
        blocks.append(far)
        blocks.append(lax.ppermute(far, "tp", swaps[0]))
    return blocks


def per_device(
    tokens, in_gain, route_ids, route_scores, gate_weight, up_weight, down_weight, out_gain
):
    count_ep = lax.axis_size("ep")
    count_tp = lax.axis_size("tp")
    experts = count_ep * gate_weight.shape[0]
    tok_count, full_width = tokens.shape
    rows = tok_count // count_tp
    start = lax.axis_index("tp") * rows
    gates = gathered(gate_weight[0], count_tp)
    ups = gathered(up_weight[0], count_tp)
    downs = gathered(down_weight[0], count_tp)
    gain_full = lax.all_gather(out_gain, "tp", axis=0, tiled=True)

    as_float = lax.dynamic_slice_in_dim(tokens, start, rows, 0).astype(jnp.float32)
    normed = (
        as_float
        * lax.rsqrt(jnp.mean(as_float * as_float, axis=1, keepdims=True) + epsilon)
        * in_gain
    ).astype(jnp.bfloat16)
    spread = lax.all_gather(normed, "ep", axis=0, tiled=True)

    ids = lax.dynamic_slice_in_dim(route_ids, start, rows, 0)
    scores = lax.dynamic_slice_in_dim(route_scores, start, rows, 0)
    mix = scores / jnp.sum(scores, axis=1, keepdims=True)
    chosen = ids[:, :, None] == jnp.arange(experts, dtype=jnp.int32)[None, None, :]
    dense = jnp.sum(jnp.where(chosen, mix[:, :, None], 0.0), axis=1).T
    weight = lax.all_to_all(dense, "ep", split_axis=0, concat_axis=0, tiled=True).reshape(-1, 1)

    def hidden_of(gate_w, up_w):
        gate_acts = jnp.dot(spread, gate_w, preferred_element_type=jnp.float32)
        up_acts = jnp.dot(spread, up_w, preferred_element_type=jnp.float32)
        return (jax.nn.silu(gate_acts) * up_acts).astype(jnp.bfloat16)

    hidden = jnp.concatenate(
        [
            hidden_of(jnp.concatenate(gates[i : i + 2], 1), jnp.concatenate(ups[i : i + 2], 1))
            for i in range(0, count_tp, 2)
        ],
        1,
    )
    expert_out = jnp.dot(
        hidden, jnp.concatenate(downs, 0), preferred_element_type=jnp.float32
    )
    terms = jnp.where(weight > 0.0, weight * expert_out, 0.0).astype(jnp.bfloat16)
    combined = lax.psum_scatter(terms, "ep", scatter_dimension=0, tiled=True).astype(jnp.float32)
    scale = lax.rsqrt(jnp.mean(combined * combined, axis=1, keepdims=True) + epsilon)
    mixed = (combined * scale * gain_full).astype(jnp.bfloat16)
    return lax.all_to_all(mixed, "tp", split_axis=1, concat_axis=0, tiled=True)


def solution(mesh):
    in_specs = (
        P("ep", None),
        P(),
        P("ep", None),
        P("ep", None),
        P("ep", None, "tp"),
        P("ep", None, "tp"),
        P("ep", "tp", None),
        P("tp"),
    )
    out_specs = P("ep", "tp")
    return jax.shard_map(
        per_device, mesh=mesh, in_specs=in_specs, out_specs=out_specs, check_vma=False
    )
```

time: 443 us -> 288 us (0.65)
  blocking collectives: 84.1 us -> 19.3 us
  waiting for transfers between devices: 249 us -> 199 us
  local copies, waits for them, and re-layouts: 43.1 us -> 2.39 us
  other arithmetic: 18 us -> 6.79 us
  starting transfers between devices: 5.85 us -> 12.6 us
  matrix products: 28.6 us -> 34.5 us
    all_to_all x1, waiting for transfers between devices: 70.4 us -> 6.13 us  [per_device(): lax.all_to_all(dense, 'ep', split_axis=0, concat_axis=0, tiled=True)]
    all_to_all x1, blocking collectives: 78.1 us -> 14.2 us  [per_device(): return lax.all_to_all(mixed, 'tp', split_axis=1, concat_axis=0, tiled=True)]
    ppermute x0 -> x9, waiting for transfers between devices: none -> 52.1 us  [the longest x3 52.1 us: gathered(): far = lax.ppermute(block, 'tp', pairs)]
    all_gather x1, waiting for transfers between devices: 81 us -> 29.9 us  [per_device(): spread = lax.all_gather(normed, 'ep', axis=0, tiled=True)]
    gather x1 -> x0, local copies, waits for them, and re-layouts: 20.5 us -> none  [per_device(): returned[flat_ids, slot_index].astype(jnp.float32)]
    unnamed x18 -> x15, local copies, waits for them, and re-layouts: 17.3 us -> 1.56 us
    reduce_scatter x1, waiting for transfers between devices: 97.3 us -> 111 us  [per_device(): lax.psum_scatter(terms, 'ep', scatter_dimension=0, tiled=True)]
    ppermute x0 -> x9, starting transfers between devices: none -> 6.15 us  [the longest x3 5.06 us: gathered(): far = lax.ppermute(block, 'tp', pairs)]
  transfers between devices with their start and end apart: 3 -> 12, of which waited for: 3 -> 6; matrix products, arithmetic and copies ran while one was open for 0% -> 8% of each run, Pallas kernels for 0% -> 0%
where the time goes in v1:
time: 288 us
  waiting for transfers between devices  199 us (69%)
  matrix products  34.5 us (12%)
  blocking collectives  19.3 us (7%)
  between operations  13.5 us (5%)
  starting transfers between devices  12.6 us (4%)
  other arithmetic  6.79 us (2%)
    reduce_scatter x1, waiting for transfers between devices, per_device(): lax.psum_scatter(terms, 'ep', scatter_dimension=0, tiled=True)  111 us
    ppermute x3, waiting for transfers between devices, gathered(): far = lax.ppermute(block, 'tp', pairs)  52.1 us
    all_gather x1, waiting for transfers between devices, per_device(): spread = lax.all_gather(normed, 'ep', axis=0, tiled=True)  29.9 us
    all_to_all x1, blocking collectives, per_device(): return lax.all_to_all(mixed, 'tp', split_axis=1, concat_axis=0, tiled=True)  14.2 us
    dot_general x1, matrix products, per_device(): jnp.dot(hidden, jnp.concatenate(downs, 0), preferred_element_type=jnp.flo...  11.8 us
    dot_general x2, matrix products, hidden_of(): gate_acts = jnp.dot(spread, gate_w, preferred_element_type=jnp.float32)  11.5 us
    dot_general x2, matrix products, hidden_of(): up_acts = jnp.dot(spread, up_w, preferred_element_type=jnp.float32)  11.3 us
    all_to_all x1, starting transfers between devices, per_device(): lax.all_to_all(dense, 'ep', split_axis=0, concat_axis=0, tiled=True)  6.36 us
  transfers between devices with their start and end apart: 12, of which 6 were waited for; matrix products, arithmetic and copies ran while one was open for 8% of the time, Pallas kernels for 0%

profile of v1, /device:TPU:0, one launch (start us, length us, event | category | flops | bytes accessed | tf_op | source)
XLA Modules:
  0.0 287.9 jit_solution(2465911979971802738)
XLA Ops:
  6.6 1.5 fusion.30
  8.1 2.3 fusion.32
  10.4 3.0 %collective-permute-start.2 = (bf16[2048,256]{1,0:T(8,128)(2,1)S(1)}, bf16[2048,256]{1,0:T(8,128)(2,1)}, u32[]{:S(2)}, u32[]{:S(2)}) collective-permute-start(bf16[2048,256]{1,0:T(8,128)(2,1)S(1)} %bitcast.25), channel_id=1, source_target_pairs={{0,2},{1,3},{2,0},{3,1},{4,6},{5,7},{6,4},{7,5},{8,10},{9,11},{10,... | collective-permute-start | bytes 3145736 | tf_op jit(solution)/shard_map/ppermute | solution.py:19
  13.6 1.9 collective-permute-start.7
  15.5 22.1 %collective-permute-done.2 = bf16[2048,256]{1,0:T(8,128)(2,1)} collective-permute-done((bf16[2048,256]{1,0:T(8,128)(2,1)S(1)}, bf16[2048,256]{1,0:T(8,128)(2,1)}, u32[]{:S(2)}, u32[]{:S(2)}) %collective-permute-start.2) | collective-permute-done | bytes 1048608 | tf_op jit(solution)/shard_map/ppermute | solution.py:19
  37.9 0.6 copy.18
  38.5 6.4 %all-to-all-start = ((f32[8,1,192]{2,1,0:T(1,128)}), f32[8,1,192]{2,1,0:T(1,128)S(1)}, u32[]{:S(2)}, u32[]{:S(2)}) async-start(f32[8,1,192]{2,1,0:T(1,128)} %copy.18), calls=%async_computation | async-start | bytes 16384 | tf_op jit(solution)/shard_map/all_to_all | solution.py:52
  45.5 6.1 %all-to-all-done = f32[8,1,192]{2,1,0:T(1,128)S(1)} async-done(((f32[8,1,192]{2,1,0:T(1,128)}), f32[8,1,192]{2,1,0:T(1,128)S(1)}, u32[]{:S(2)}, u32[]{:S(2)}) %all-to-all-start) | async-done | bytes 6176 | tf_op jit(solution)/shard_map/all_to_all | solution.py:52
  51.7 8.4 %collective-permute-done.4 = bf16[2048,256]{1,0:T(8,128)(2,1)} collective-permute-done((bf16[2048,256]{1,0:T(8,128)(2,1)S(1)}, bf16[2048,256]{1,0:T(8,128)(2,1)}, u32[]{:S(2)}, u32[]{:S(2)}) %collective-permute-start.4) | collective-permute-done | bytes 1048608 | tf_op jit(solution)/shard_map/ppermute | solution.py:19
  60.1 21.6 %collective-permute-done.7 = bf16[256,2048]{1,0:T(8,128)(2,1)} collective-permute-done((bf16[256,2048]{1,0:T(8,128)(2,1)S(1)}, bf16[256,2048]{1,0:T(8,128)(2,1)}, u32[]{:S(2)}, u32[]{:S(2)}) %collective-permute-start.7) | collective-permute-done | bytes 1048608 | tf_op jit(solution)/shard_map/ppermute | solution.py:19
  81.7 0.5 collective-permute-start.8
  82.2 29.9 %all-gather.3.cloned.1.call-done = bf16[1536,2048]{1,0:T(8,128)(2,1)} async-done(((bf16[192,2048]{1,0:T(8,128)(2,1)}), bf16[1536,2048]{1,0:T(8,128)(2,1)}) %all-gather.3.cloned.1.call-update) | async-done | bytes 6291472 | tf_op jit(solution)/shard_map/all_gather | solution.py:45
  112.1 6.6 %fusion.20 = f32[1536,512]{0,1:T(8,128)S(1)} fusion(bf16[1536,2048]{1,0:T(8,128)(2,1)} %all-gather.3.cloned.1.call-done, bf16[2048,256]{1,0:T(8,128)(2,1)} %collective-permute-done.3, bf16[2048,256]{1,0:T(8,128)(2,1)} %collective-permute-done.2), kind=kOutput, calls=%fused_computation.21 | convolution fusion | flops 3225419776 | bytes 11534336 | tf_op jit(solution)/shard_map/dot_general | solution.py:55
  118.7 4.9 %fusion.10 = f32[1536,512]{0,1:T(8,128)S(1)} fusion(bf16[1536,2048]{1,0:T(8,128)(2,1)S(1)} %copy-done.3, bf16[2048,256]{1,0:T(8,128)(2,1)} %collective-permute-done, bf16[2048,256]{1,0:T(8,128)(2,1)S(1)} %bitcast.27), kind=kOutput, calls=%fused_computation.13 | convolution fusion | flops 3225419776 | bytes 11534336 | tf_op jit(solution)/shard_map/dot_general | solution.py:55
  123.7 5.8 %multiply_convert_fusion = bf16[1536,512]{0,1:T(8,128)(2,1)S(1)} fusion(f32[1536,512]{0,1:T(8,128)S(1)} %fusion.20, bf16[1536,2048]{1,0:T(8,128)(2,1)S(1)} %copy-done.3, bf16[2048,256]{1,0:T(8,128)(2,1)} %collective-permute-done.5, bf16[2048,256]{1,0:T(8,128)(2,1)} %collective-permute-done.4), kind=kOutput, calls=%fused_computation.11 | convolution fusion | flops 3230138368 | bytes 13107200 | tf_op jit(solution)/shard_map/dot_general | solution.py:56
  129.5 5.5 %multiply_convert_fusion.1 = bf16[1536,512]{0,1:T(8,128)(2,1)S(1)} fusion(f32[1536,512]{0,1:T(8,128)S(1)} %fusion.10, bf16[1536,2048]{1,0:T(8,128)(2,1)S(1)} %copy-done.3, bf16[2048,256]{1,0:T(8,128)(2,1)} %collective-permute-done.1, bf16[2048,256]{1,0:T(8,128)(2,1)S(1)} %bitcast.30), kind=kOutput, calls=%fused_computation.12 | convolution fusion | flops 3230138368 | bytes 13107200 | tf_op jit(solution)/shard_map/dot_general | solution.py:56
  135.0 11.8 %select_convert_fusion = bf16[1536,2048]{1,0:T(8,128)(2,1)} fusion(f32[1536]{0:T(1024)S(1)} %reshape.39, pred[1536]{0:T(1024)(128)(4,1)S(1)} %broadcast_compare_fusion, bf16[256,2048]{1,0:T(8,128)(2,1)} %collective-permute-done.8, bf16[256,2048]{1,0:T(8,128)(2,1)} %collective-permute-done.7, bf16[256,2048]{1,0:T(8,128)(2,1)} %collective-permute-done.6, ...), kind=kOutput, calls=%fused_computation | convolution fusion | flops 6474956800 | bytes 13639168 | tf_op jit(solution)/shard_map/dot_general | solution.py:66
  146.8 0.7 copy-done.2
  147.5 5.2 %all-gather = f32[4,1,512]{2,1,0:T(1,128)S(1)} all-gather(f32[1,1,512]{2,1,0:T(1,128)S(1)} %bitcast.24), channel_id=1, replica_groups=mesh['ep'=8,'tp'=4] {'tp'}, dimensions={0}, use_global_device_ids=true | all-gather | bytes 10240 | tf_op jit(solution)/shard_map/all_gather | solution.py:37
  152.6 110.5 %reduce-scatter.2.cloned.1.call-done = bf16[192,2048]{1,0:T(8,128)(2,1)} async-done(((bf16[1536,2048]{1,0:T(8,128)(2,1)}), bf16[192,2048]{1,0:T(8,128)(2,1)}) %reduce-scatter.2.cloned.1.call-update) | async-done | bytes 786448 | tf_op jit(solution)/shard_map/reduce_scatter | solution.py:70
  263.2 1.4 fusion.33
  264.5 1.4 fusion.35
  266.0 14.2 %all_to_all.28 = bf16[192,4,512]{2,0,1:T(8,128)(2,1)S(1)} all-to-all(bf16[192,4,512]{2,0,1:T(8,128)(2,1)S(1)} %bitcast.19), channel_id=1, replica_groups=mesh['ep'=8,'tp'=4] {'tp'}, dimensions={1} | all-to-all | bytes 1572864 | tf_op jit(solution)/shard_map/all_to_all | solution.py:73
  280.2 0.9 copy.24
  (39 shorter events, 1.3 us)
Async XLA Ops:
  6.5 31.2 %copy-start = (s32[768,2]{0,1:T(2,128)S(1)}, s32[768,2]{0,1:T(2,128)}, u32[]{:S(2)}) copy-start(s32[768,2]{0,1:T(2,128)} %param.10) | copy-start | bytes 18436
  6.5 3.9 %copy-start.4 = (bf16[1,2048,256]{2,1,0:T(8,128)(2,1)S(1)}, bf16[1,2048,256]{2,1,0:T(8,128)(2,1)}, u32[]{:S(2)}) copy-start(bf16[1,2048,256]{2,1,0:T(8,128)(2,1)} %param.12) | copy-start | bytes 3145732
  6.5 6.9 %copy-start.5 = (bf16[1,2048,256]{2,1,0:T(8,128)(2,1)S(1)}, bf16[1,2048,256]{2,1,0:T(8,128)(2,1)}, u32[]{:S(2)}) copy-start(bf16[1,2048,256]{2,1,0:T(8,128)(2,1)} %param.13) | copy-start | bytes 3145732
  6.5 7.0 %copy-start.6 = (bf16[1,256,2048]{2,1,0:T(8,128)(2,1)S(1)}, bf16[1,256,2048]{2,1,0:T(8,128)(2,1)}, u32[]{:S(2)}) copy-start(bf16[1,256,2048]{2,1,0:T(8,128)(2,1)} %param.14) | copy-start | bytes 3145732
  6.5 31.1 %copy-start.1 = (f32[768,2]{0,1:T(2,128)S(1)}, f32[768,2]{0,1:T(2,128)}, u32[]{:S(2)}) copy-start(f32[768,2]{0,1:T(2,128)} %param.11) | copy-start | bytes 18436
  6.5 105.6 %all-gather.3.cloned.1.call-start = ((), (), s32[]{:S(2)}) async-start(), calls=%async_computation.3 | async-start | bytes 7077888 | tf_op jit(solution)/shard_map/all_gather | solution.py:45
  10.4 27.1 %collective-permute-start.2 = (bf16[2048,256]{1,0:T(8,128)(2,1)S(1)}, bf16[2048,256]{1,0:T(8,128)(2,1)}, u32[]{:S(2)}, u32[]{:S(2)}) collective-permute-start(bf16[2048,256]{1,0:T(8,128)(2,1)S(1)} %bitcast.25), channel_id=1, source_target_pairs={{0,2},{1,3},{2,0},{3,1},{4,6},{5,7},{6,4},{7,5},{8,10},{9,11},{10,... | collective-permute-start | bytes 3145736 | tf_op jit(solution)/shard_map/ppermute | solution.py:19
  13.5 46.6 %collective-permute-start.4 = (bf16[2048,256]{1,0:T(8,128)(2,1)S(1)}, bf16[2048,256]{1,0:T(8,128)(2,1)}, u32[]{:S(2)}, u32[]{:S(2)}) collective-permute-start(bf16[2048,256]{1,0:T(8,128)(2,1)S(1)} %bitcast.28), channel_id=1, source_target_pairs={{0,2},{1,3},{2,0},{3,1},{4,6},{5,7},{6,4},{7,5},{8,10},{9,11},{10,... | collective-permute-start | bytes 3145736 | tf_op jit(solution)/shard_map/ppermute | solution.py:19
  13.6 68.1 %collective-permute-start.7 = (bf16[256,2048]{1,0:T(8,128)(2,1)S(1)}, bf16[256,2048]{1,0:T(8,128)(2,1)}, u32[]{:S(2)}, u32[]{:S(2)}) collective-permute-start(bf16[256,2048]{1,0:T(8,128)(2,1)S(1)} %bitcast.31), channel_id=1, source_target_pairs={{0,2},{1,3},{2,0},{3,1},{4,6},{5,7},{6,4},{7,5},{8,10},{9,11},{10,... | collective-permute-start | bytes 3145736 | tf_op jit(solution)/shard_map/ppermute | solution.py:19
  37.6 44.1 %collective-permute-start.3 = (bf16[2048,256]{1,0:T(8,128)(2,1)}, bf16[2048,256]{1,0:T(8,128)(2,1)}, u32[]{:S(2)}, u32[]{:S(2)}) collective-permute-start(bf16[2048,256]{1,0:T(8,128)(2,1)} %collective-permute-done.2), channel_id=1, source_target_pairs={{0,1},{1,0},{2,3},{3,2},{4,5},{5,4},{6,7},{7,6},{8,9},{9,8},{10,11... | collective-permute-start | bytes 3145736 | tf_op jit(solution)/shard_map/ppermute | solution.py:21
  38.5 13.1 %all-to-all-start = ((f32[8,1,192]{2,1,0:T(1,128)}), f32[8,1,192]{2,1,0:T(1,128)S(1)}, u32[]{:S(2)}, u32[]{:S(2)}) async-start(f32[8,1,192]{2,1,0:T(1,128)} %copy.18), calls=%async_computation | async-start | bytes 16384 | tf_op jit(solution)/shard_map/all_to_all | solution.py:52
  44.8 218.3 %reduce-scatter.2.cloned.1.call-start = ((), (), s32[]{:S(2)}) async-start(), calls=%async_computation.4 | async-start | bytes 7077888 | tf_op jit(solution)/shard_map/reduce_scatter | solution.py:70
  44.9 73.8 %collective-permute-start = (bf16[2048,256]{1,0:T(8,128)(2,1)S(1)}, bf16[2048,256]{1,0:T(8,128)(2,1)}, u32[]{:S(2)}, u32[]{:S(2)}) collective-permute-start(bf16[2048,256]{1,0:T(8,128)(2,1)S(1)} %bitcast.26), channel_id=1, source_target_pairs={{0,1},{1,0},{2,3},{3,2},{4,5},{5,4},{6,7},{7,6},{8,9},{9,8},{10,11... | collective-permute-start | bytes 3145736 | tf_op jit(solution)/shard_map/ppermute | solution.py:16
  45.2 84.3 %collective-permute-start.1 = (bf16[2048,256]{1,0:T(8,128)(2,1)S(1)}, bf16[2048,256]{1,0:T(8,128)(2,1)}, u32[]{:S(2)}, u32[]{:S(2)}) collective-permute-start(bf16[2048,256]{1,0:T(8,128)(2,1)S(1)} %bitcast.29), channel_id=1, source_target_pairs={{0,1},{1,0},{2,3},{3,2},{4,5},{5,4},{6,7},{7,6},{8,9},{9,8},{10,11... | collective-permute-start | bytes 3145736 | tf_op jit(solution)/shard_map/ppermute | solution.py:16
  60.1 74.9 %collective-permute-start.6 = (bf16[256,2048]{1,0:T(8,128)(2,1)S(1)}, bf16[256,2048]{1,0:T(8,128)(2,1)}, u32[]{:S(2)}, u32[]{:S(2)}) collective-permute-start(bf16[256,2048]{1,0:T(8,128)(2,1)S(1)} %bitcast.32), channel_id=1, source_target_pairs={{0,1},{1,0},{2,3},{3,2},{4,5},{5,4},{6,7},{7,6},{8,9},{9,8},{10,11... | collective-permute-start | bytes 3145736 | tf_op jit(solution)/shard_map/ppermute | solution.py:16
  81.7 42.0 %collective-permute-start.5 = (bf16[2048,256]{1,0:T(8,128)(2,1)}, bf16[2048,256]{1,0:T(8,128)(2,1)}, u32[]{:S(2)}, u32[]{:S(2)}) collective-permute-start(bf16[2048,256]{1,0:T(8,128)(2,1)} %collective-permute-done.4), channel_id=1, source_target_pairs={{0,1},{1,0},{2,3},{3,2},{4,5},{5,4},{6,7},{7,6},{8,9},{9,8},{10,11... | collective-permute-start | bytes 3145736 | tf_op jit(solution)/shard_map/ppermute | solution.py:21
  81.7 53.3 %collective-permute-start.8 = (bf16[256,2048]{1,0:T(8,128)(2,1)}, bf16[256,2048]{1,0:T(8,128)(2,1)}, u32[]{:S(2)}, u32[]{:S(2)}) collective-permute-start(bf16[256,2048]{1,0:T(8,128)(2,1)} %collective-permute-done.7), channel_id=1, source_target_pairs={{0,1},{1,0},{2,3},{3,2},{4,5},{5,4},{6,7},{7,6},{8,9},{9,8},{10,11... | collective-permute-start | bytes 3145736 | tf_op jit(solution)/shard_map/ppermute | solution.py:21
  112.1 6.6 %copy-start.3 = (bf16[1536,2048]{1,0:T(8,128)(2,1)S(1)}, bf16[1536,2048]{1,0:T(8,128)(2,1)}, u32[]{:S(2)}) copy-start(bf16[1536,2048]{1,0:T(8,128)(2,1)} %all-gather.3.cloned.1.call-done) | copy-start | bytes 18874372
  146.8 0.7 copy-start.2
Sparse Core Ops, SparseCore 0:
  10.6 101.5 all-gather.2
  146.9 116.1 reduce-scatter.1
